TPU v7x, 32 devices: a whole 2x2x4 slice. The times are simulated.
32 devices in a mesh: fs: 8 (over z, x), tp: 4 (over y, core).
Axes of the slice: x: 2, y: 2, z: 4, core: 2. Of those that a mesh axis runs over, the one named last changes fastest.
Arguments:
- prompt_rows: bfloat16 [512, 3072], P('tp'), may hold values from -6 to 6
- gate_first: float32 [3072, 8192], P('fs', 'tp'), may hold values from -0.109375 to 0.109375
- up_first: float32 [3072, 8192], P('fs', 'tp'), may hold values from -0.109375 to 0.109375
- down_first: float32 [8192, 3072], P('fs', 'tp'), may hold values from -0.0625 to 0.0625
- gate_second: float32 [3072, 8192], P('fs', 'tp'), may hold values from -0.109375 to 0.109375
- up_second: float32 [3072, 8192], P('fs', 'tp'), may hold values from -0.109375 to 0.109375
- down_second: float32 [8192, 3072], P('fs', 'tp'), may hold values from -0.0625 to 0.0625
- pre_gain_first: float32 [3072], replicated, may hold values from 0.1 to 1.9
- post_gain_first: float32 [3072], replicated, may hold values from 0.1 to 1.9
- pre_gain_second: float32 [3072], replicated, may hold values from 0.1 to 1.9
- post_gain_second: float32 [3072], replicated, may hold values from 0.1 to 1.9
Outputs:
- result_rows: bfloat16 [512, 3072], P('tp')
- gate_first_new: bfloat16 [3072, 8192], P(None, 'fs')
- up_first_new: bfloat16 [3072, 8192], P(None, 'fs')
- down_first_new: bfloat16 [8192, 3072], P('fs')
- gate_second_new: bfloat16 [3072, 8192], P(None, 'fs')
- up_second_new: bfloat16 [3072, 8192], P(None, 'fs')
- down_second_new: bfloat16 [8192, 3072], P('fs')
All inputs are finite; a program needn't handle non-finite values.
Results may differ from a plain program's by a relative error of at most 0.0071.
Values may be sent and summed in bfloat16 or wider, within the bound.
A program may use at most 192 MiB of HBM per device.

v0:
```python
import jax
import jax.numpy as jnp
from jax import lax
from jax.sharding import PartitionSpec as P

EPSILON = 1e-06


def half_step(rows, gate, up, down, post_gain):
    floats = rows.astype(jnp.float32)
    normed = (
        floats * lax.rsqrt(jnp.mean(floats * floats, axis=-1, keepdims=True) + EPSILON)
    ).astype(jnp.bfloat16)
    gate_pre = jnp.dot(normed, gate, preferred_element_type=jnp.float32)
    up_pre = jnp.dot(normed, up, preferred_element_type=jnp.float32)
    hidden = (jax.nn.silu(gate_pre) * up_pre).astype(jnp.bfloat16)
    partial_value = jnp.dot(hidden, down, preferred_element_type=jnp.float32)
    total = lax.psum(partial_value, "fs")
    scale = lax.rsqrt(jnp.mean(total * total, axis=-1, keepdims=True) + EPSILON)
    return (floats + 0.5 * total * scale * post_gain[None, :]).astype(jnp.bfloat16)


def per_device(
    prompt_rows,
    gate_first,
    up_first,
    down_first,
    gate_second,
    up_second,
    down_second,
    pre_gain_first,
    post_gain_first,
    pre_gain_second,
    post_gain_second,
):
    height = gate_first.shape[0]
    start = lax.axis_index("fs") * height
    gain_a = lax.dynamic_slice_in_dim(pre_gain_first, start, height, 0)[:, None]
    gain_b = lax.dynamic_slice_in_dim(pre_gain_second, start, height, 0)[:, None]
    wide = (
        lax.all_gather((gain_a * gate_first).astype(jnp.bfloat16), "tp", axis=1, tiled=True),
        lax.all_gather((gain_a * up_first).astype(jnp.bfloat16), "tp", axis=1, tiled=True),
        lax.all_gather(down_first.astype(jnp.bfloat16), "tp", axis=1, tiled=True),
        lax.all_gather((gain_b * gate_second).astype(jnp.bfloat16), "tp", axis=1, tiled=True),
        lax.all_gather((gain_b * up_second).astype(jnp.bfloat16), "tp", axis=1, tiled=True),
        lax.all_gather(down_second.astype(jnp.bfloat16), "tp", axis=1, tiled=True),
    )
    gate_a, up_a, gate_b, up_b = (
        lax.all_to_all(wide[0], "fs", split_axis=1, concat_axis=0, tiled=True),
        lax.all_to_all(wide[1], "fs", split_axis=1, concat_axis=0, tiled=True),
        lax.all_to_all(wide[3], "fs", split_axis=1, concat_axis=0, tiled=True),
        lax.all_to_all(wide[4], "fs", split_axis=1, concat_axis=0, tiled=True),
    )
    down_a = wide[2]
    down_b = wide[5]
    middle = half_step(prompt_rows, gate_a, up_a, down_a, post_gain_first)
    result = half_step(middle, gate_b, up_b, down_b, post_gain_second)
    return (result, gate_a, up_a, down_a, gate_b, up_b, down_b)


def solution(mesh):
    return jax.shard_map(
        per_device,
        mesh=mesh,
        in_specs=(
            P("tp", None),
            P("fs", "tp"),
            P("fs", "tp"),
            P("fs", "tp"),
            P("fs", "tp"),
            P("fs", "tp"),
            P("fs", "tp"),
            P(),
            P(),
            P(),
            P(),
        ),
        out_specs=(
            P("tp", None),
            P(None, "fs"),
            P(None, "fs"),
            P("fs", None),
            P(None, "fs"),
            P(None, "fs"),
            P("fs", None),
        ),
        check_vma=False,
    )
```

profile of v0, /device:TPU:0, one launch (start us, length us, event | category | flops | bytes accessed | tf_op | source)
XLA Modules:
  0.0 843.3 jit_solution(3647729259422297711)
XLA Ops:
  8.0 5.5 multiply_convert_fusion.3
  14.3 48.5 %all-gather.7.cloned.1.call-done = bf16[384,8192]{1,0:T(8,128)(2,1)} async-done(((bf16[384,2048]{1,0:T(8,128)(2,1)}), bf16[384,8192]{1,0:T(8,128)(2,1)}) %all-gather.7.cloned.1.call-update) | async-done | bytes 6291472 | tf_op jit(solution)/shard_map/all_gather | solution.py:41
  62.7 6.5 copy.33
  69.2 5.8 all-to-all-start
  80.4 30.9 %all-gather.9.cloned.1.call-done = bf16[384,8192]{1,0:T(8,128)(2,1)} async-done(((bf16[384,2048]{1,0:T(8,128)(2,1)}), bf16[384,8192]{1,0:T(8,128)(2,1)}) %all-gather.9.cloned.1.call-update) | async-done | bytes 6291472 | tf_op jit(solution)/shard_map/all_gather | solution.py:42
  111.3 6.5 copy.32
  117.8 95.9 %all-to-all-done = bf16[384,8,1024]{2,0,1:T(8,128)(2,1)} async-done(((bf16[384,8,1024]{2,0,1:T(8,128)(2,1)}), bf16[384,8,1024]{2,0,1:T(8,128)(2,1)}, u32[]{:S(2)}, u32[]{:S(2)}) %all-to-all-start) | async-done | bytes 6291488 | tf_op jit(solution)/shard_map/all_to_all | solution.py:49
  213.7 4.8 all-to-all-start.1
  219.0 6.5 copy.31
  225.5 130.6 %all-to-all-done.1 = bf16[384,8,1024]{2,0,1:T(8,128)(2,1)} async-done(((bf16[384,8,1024]{2,0,1:T(8,128)(2,1)}), bf16[384,8,1024]{2,0,1:T(8,128)(2,1)}, u32[]{:S(2)}, u32[]{:S(2)}) %all-to-all-start.1) | async-done | bytes 6291488 | tf_op jit(solution)/shard_map/all_to_all | solution.py:50
  356.1 4.8 all-to-all-start.2
  364.6 6.5 copy.30
  375.7 35.5 %all-gather.11.cloned.1.call-done = bf16[1024,3072]{1,0:T(8,128)(2,1)} async-done(((bf16[1024,768]{1,0:T(8,128)(2,1)}), bf16[1024,3072]{1,0:T(8,128)(2,1)}) %all-gather.11.cloned.1.call-update) | async-done | bytes 6291472 | tf_op jit(solution)/shard_map/all_gather | solution.py:43
  411.2 7.7 fusion.9
  418.9 100.4 %all-to-all-done.2 = bf16[384,8,1024]{2,0,1:T(8,128)(2,1)} async-done(((bf16[384,8,1024]{2,0,1:T(8,128)(2,1)}), bf16[384,8,1024]{2,0,1:T(8,128)(2,1)}, u32[]{:S(2)}, u32[]{:S(2)}) %all-to-all-start.2) | async-done | bytes 6291488 | tf_op jit(solution)/shard_map/all_to_all | solution.py:51
  519.3 4.8 all-to-all-start.3
  527.7 130.8 %all-reduce.3.cloned.1.call-done = f32[128,3072]{1,0:T(8,128)} async-done(((f32[128,3072]{1,0:T(8,128)}), f32[128,3072]{1,0:T(8,128)}) %all-reduce.3.cloned.1.call-update) | async-done | bytes 1572880 | tf_op jit(solution)/shard_map/psum | solution.py:18
  666.3 38.0 %all-gather.17.cloned.1.call-done = bf16[1024,3072]{1,0:T(8,128)(2,1)} async-done(((bf16[1024,768]{1,0:T(8,128)(2,1)}), bf16[1024,3072]{1,0:T(8,128)(2,1)}) %all-gather.17.cloned.1.call-update) | async-done | bytes 6291472 | tf_op jit(solution)/shard_map/all_gather | solution.py:46
  704.2 7.7 fusion.8
  712.0 89.4 %all-reduce.5.cloned.1.call-done = f32[128,3072]{1,0:T(8,128)} async-done(((f32[128,3072]{1,0:T(8,128)}), f32[128,3072]{1,0:T(8,128)}) %all-reduce.5.cloned.1.call-update) | async-done | bytes 1572880 | tf_op jit(solution)/shard_map/psum | solution.py:18
  805.6 6.4 copy.42
  812.0 6.3 copy.43
  821.0 6.4 copy.45
  827.4 6.3 copy.46
  (55 shorter events, 36.7 us)
Async XLA Ops:
  7.2 55.6 %all-gather.7.cloned.1.call-start = ((), (), s32[]{:S(2)}) async-start(), calls=%async_computation.4 | async-start | bytes 7864320 | tf_op jit(solution)/shard_map/all_gather | solution.py:41
  13.5 97.8 %all-gather.9.cloned.1.call-start = ((), (), s32[]{:S(2)}) async-start(), calls=%async_computation.5 | async-start | bytes 7864320 | tf_op jit(solution)/shard_map/all_gather | solution.py:42
  69.2 6.6 copy-start.1
  69.2 144.4 %all-to-all-start = ((bf16[384,8,1024]{2,0,1:T(8,128)(2,1)}), bf16[384,8,1024]{2,0,1:T(8,128)(2,1)}, u32[]{:S(2)}, u32[]{:S(2)}) async-start(bf16[384,8,1024]{2,0,1:T(8,128)(2,1)} %bitcast.40), calls=%async_computation | async-start | bytes 12582912 | tf_op jit(solution)/shard_map/all_to_all | solution.py:49
  75.0 144.0 %all-gather.13.cloned.1.call-start = ((), (), s32[]{:S(2)}) async-start(), calls=%async_computation.8 | async-start | bytes 7864320 | tf_op jit(solution)/shard_map/all_gather | solution.py:44
  213.7 142.5 %all-to-all-start.1 = ((bf16[384,8,1024]{2,0,1:T(8,128)(2,1)}), bf16[384,8,1024]{2,0,1:T(8,128)(2,1)}, u32[]{:S(2)}, u32[]{:S(2)}) async-start(bf16[384,8,1024]{2,0,1:T(8,128)(2,1)} %bitcast.41), calls=%async_computation.1 | async-start | bytes 12582912 | tf_op jit(solution)/shard_map/all_to_all | solution.py:50
  218.4 146.2 %all-gather.15.cloned.1.call-start = ((), (), s32[]{:S(2)}) async-start(), calls=%async_computation.9 | async-start | bytes 7864320 | tf_op jit(solution)/shard_map/all_gather | solution.py:45
  356.1 163.1 %all-to-all-start.2 = ((bf16[384,8,1024]{2,0,1:T(8,128)(2,1)}), bf16[384,8,1024]{2,0,1:T(8,128)(2,1)}, u32[]{:S(2)}, u32[]{:S(2)}) async-start(bf16[384,8,1024]{2,0,1:T(8,128)(2,1)} %bitcast.39), calls=%async_computation.2 | async-start | bytes 12582912 | tf_op jit(solution)/shard_map/all_to_all | solution.py:51
  361.0 3.4 copy-start
  361.0 50.2 %all-gather.11.cloned.1.call-start = ((), (), s32[]{:S(2)}) async-start(), calls=%async_computation.6 | async-start | bytes 7864320 | tf_op jit(solution)/shard_map/all_gather | solution.py:43
  364.3 294.2 %all-reduce.3.cloned.1.call-start = ((), (), s32[]{:S(2)}) async-start(), calls=%async_computation.7 | async-start | bytes 3145728 | tf_op jit(solution)/shard_map/psum | solution.py:18
  519.3 185.0 %all-to-all-start.3 = ((bf16[384,8,1024]{2,0,1:T(8,128)(2,1)}), bf16[384,8,1024]{2,0,1:T(8,128)(2,1)}, u32[]{:S(2)}, u32[]{:S(2)}) async-start(bf16[384,8,1024]{2,0,1:T(8,128)(2,1)} %bitcast.38), calls=%async_computation.3 | async-start | bytes 12582912 | tf_op jit(solution)/shard_map/all_to_all | solution.py:52
  524.1 136.0 %copy-start.2 = (f32[3072]{0:T(1024)S(1)}, f32[3072]{0:T(1024)}, u32[]{:S(2)}) copy-start(f32[3072]{0:T(1024)} %param.19) | copy-start | bytes 36868
  524.1 180.1 %all-gather.17.cloned.1.call-start = ((), (), s32[]{:S(2)}) async-start(), calls=%async_computation.10 | async-start | bytes 7864320 | tf_op jit(solution)/shard_map/all_gather | solution.py:46
  527.4 273.9 %all-reduce.5.cloned.1.call-start = ((), (), s32[]{:S(2)}) async-start(), calls=%async_computation.11 | async-start | bytes 3145728 | tf_op jit(solution)/shard_map/psum | solution.py:18
  711.9 91.1 %copy-start.3 = (f32[3072]{0:T(1024)S(1)}, f32[3072]{0:T(1024)}, u32[]{:S(2)}) copy-start(f32[3072]{0:T(1024)} %param.21) | copy-start | bytes 36868
  805.6 12.7 %slice-start = ((s8[6291456]{0:T(1024)(128)(4,1)}), s8[4194304]{0:T(1024)(128)(4,1)S(1)}, s32[]{:S(2)}) async-start(s8[6291456]{0:T(1024)(128)(4,1)} %bitcast.34), calls=%async_computation.12 | async-start | bytes 8388608
  812.0 6.4 slice-start.1
  821.0 12.7 %slice-start.2 = ((s8[6291456]{0:T(1024)(128)(4,1)}), s8[4194304]{0:T(1024)(128)(4,1)S(1)}, s32[]{:S(2)}) async-start(s8[6291456]{0:T(1024)(128)(4,1)} %bitcast.36), calls=%async_computation.14 | async-start | bytes 8388608
  827.4 6.4 slice-start.3
Sparse Core Ops, SparseCore 0:
  13.6 49.0 all-gather.6
  64.9 46.3 all-gather.8
  113.4 46.3 all-gather.12
  221.1 46.7 all-gather.14
  364.4 46.6 all-gather.10
  419.0 239.4 all-reduce.2
  660.6 43.5 all-gather.16
  712.1 89.2 all-reduce.4
where the time goes:
time: 844 us; the launch traced here: 843 us
  waiting for transfers between devices  701 us (83%)
  local copies, waits for them, and re-layouts  58.5 us (7%)
  other arithmetic  24.5 us (3%)
  matrix products  24.2 us (3%)
  starting transfers between devices  20.7 us (2%)
  between operations  14.3 us (2%)
    psum x2, waiting for transfers between devices, half_step(): total = lax.psum(partial_value, 'fs')  220 us
    all_to_all x1, waiting for transfers between devices, per_device(): lax.all_to_all(wide[1], 'fs', split_axis=1, concat_axis=0, tiled=True)  131 us
    all_to_all x1, waiting for transfers between devices, per_device(): lax.all_to_all(wide[3], 'fs', split_axis=1, concat_axis=0, tiled=True)  100 us
    all_to_all x1, waiting for transfers between devices, per_device(): lax.all_to_all(wide[0], 'fs', split_axis=1, concat_axis=0, tiled=True)  95.9 us
    all_gather x1, waiting for transfers between devices, per_device(): lax.all_gather((gain_a * gate_first).astype(jnp.bfloat16), 'tp', axis=1,...  48.5 us
    all_gather x1, waiting for transfers between devices, per_device(): lax.all_gather(down_second.astype(jnp.bfloat16), 'tp', axis=1, tiled=True)  38 us
    all_gather x1, waiting for transfers between devices, per_device(): lax.all_gather(down_first.astype(jnp.bfloat16), 'tp', axis=1, tiled=True)  35.5 us
    unnamed x22, local copies, waits for them, and re-layouts  30.9 us
  transfers between devices with their start and end apart: 12, of which 9 were waited for; matrix products, arithmetic and copies ran while one was open for 7% of the time, Pallas kernels for 0%

commit v1 on v0

--- a/solution.py
+++ b/solution.py
@@ -1,9 +1,25 @@
+import functools
 import jax
 import jax.numpy as jnp
 from jax import lax
 from jax.sharding import PartitionSpec as P
 
 EPSILON = 1e-06
+
+
+def play_the_figure(own_rows, peer_axis):
+    n_axis = lax.psum(1, axis_name=peer_axis)
+    now, formed = (own_rows, 0)
+    while 1 << formed < n_axis:
+        step_out = lax.ppermute(
+            now, axis_name=peer_axis, perm=tuple(((j, j ^ 1 << formed) for j in range(n_axis)))
+        )
+        now = now + step_out
+        formed = formed + 1
+    return now
+
+
+kinds_point = functools.partial(play_the_figure, peer_axis="fs")
 
 
 def half_step(rows, gate, up, down, post_gain):
@@ -15,7 +31,7 @@
     up_pre = jnp.dot(normed, up, preferred_element_type=jnp.float32)
     hidden = (jax.nn.silu(gate_pre) * up_pre).astype(jnp.bfloat16)
     partial_value = jnp.dot(hidden, down, preferred_element_type=jnp.float32)
-    total = lax.psum(partial_value, "fs")
+    total = kinds_point(partial_value)
     scale = lax.rsqrt(jnp.mean(total * total, axis=-1, keepdims=True) + EPSILON)
     return (floats + 0.5 * total * scale * post_gain[None, :]).astype(jnp.bfloat16)
 

time: 844 us -> 936 us (1.11)
  waiting for transfers between devices: 701 us -> 793 us
  starting transfers between devices: 20.7 us -> 30.5 us
    ppermute x0 -> x6, waiting for transfers between devices: none -> 357 us  [play_the_figure(): lax.ppermute(now, axis_name=peer_axis, perm=tuple(((j, j ^ 1 << formed) f...]
    psum x2 -> x0, waiting for transfers between devices: 220 us -> none  [half_step(): total = lax.psum(partial_value, 'fs')]
    all_gather x1, waiting for transfers between devices: 38 us -> 0.02 us  [per_device(): lax.all_gather(down_second.astype(jnp.bfloat16), 'tp', axis=1, tiled=True)]
    all_gather x1, waiting for transfers between devices: 35.5 us -> 0.02 us  [per_device(): lax.all_gather(down_first.astype(jnp.bfloat16), 'tp', axis=1, tiled=True)]
    all_to_all x1, waiting for transfers between devices: 100 us -> 129 us  [per_device(): lax.all_to_all(wide[3], 'fs', split_axis=1, concat_axis=0, tiled=True)]
    ppermute x0 -> x6, starting transfers between devices: none -> 9.54 us  [play_the_figure(): lax.ppermute(now, axis_name=peer_axis, perm=tuple(((j, j ^ 1 << formed) f...]
    unnamed x22 -> x26, local copies, waits for them, and re-layouts: 30.9 us -> 32 us
  transfers between devices with their start and end apart: 12 -> 16, of which waited for: 9 -> 11; matrix products, arithmetic and copies ran while one was open for 7% -> 5% of each run, Pallas kernels for 0% -> 0%
where the time goes in v1:
time: 936 us
  waiting for transfers between devices  793 us (85%)
  local copies, waits for them, and re-layouts  59.6 us (6%)
  starting transfers between devices  30.5 us (3%)
  matrix products  21.9 us (2%)
  other arithmetic  16 us (2%)
  between operations  14.3 us (2%)
    ppermute x6, waiting for transfers between devices, play_the_figure(): lax.ppermute(now, axis_name=peer_axis, perm=tuple(((j, j ^ 1 << formed) f...  357 us
    all_to_all x1, waiting for transfers between devices, per_device(): lax.all_to_all(wide[1], 'fs', split_axis=1, concat_axis=0, tiled=True)  131 us
    all_to_all x1, waiting for transfers between devices, per_device(): lax.all_to_all(wide[3], 'fs', split_axis=1, concat_axis=0, tiled=True)  129 us
    all_to_all x1, waiting for transfers between devices, per_device(): lax.all_to_all(wide[0], 'fs', split_axis=1, concat_axis=0, tiled=True)  95.9 us
    all_gather x1, waiting for transfers between devices, per_device(): lax.all_gather((gain_a * gate_first).astype(jnp.bfloat16), 'tp', axis=1,...  48.5 us
    unnamed x26, local copies, waits for them, and re-layouts  32 us
    all_gather x1, waiting for transfers between devices, per_device(): lax.all_gather((gain_a * up_first).astype(jnp.bfloat16), 'tp', axis=1, ti...  30.9 us
  transfers between devices with their start and end apart: 16, of which 11 were waited for; matrix products, arithmetic and copies ran while one was open for 5% of the time, Pallas kernels for 0%

profile of v1, /device:TPU:0, one launch (start us, length us, event | category | flops | bytes accessed | tf_op | source)
XLA Modules:
  0.0 935.5 jit_solution(4626363899245537802)
XLA Ops:
  8.0 5.5 multiply_convert_fusion.3
  14.3 48.5 %all-gather.7.cloned.1.call-done = bf16[384,8192]{1,0:T(8,128)(2,1)} async-done(((bf16[384,2048]{1,0:T(8,128)(2,1)}), bf16[384,8192]{1,0:T(8,128)(2,1)}) %all-gather.7.cloned.1.call-update) | async-done | bytes 6291472 | tf_op jit(solution)/shard_map/all_gather | solution.py:57
  62.7 6.5 copy.33
  69.2 5.8 all-to-all-start
  80.4 30.9 %all-gather.9.cloned.1.call-done = bf16[384,8192]{1,0:T(8,128)(2,1)} async-done(((bf16[384,2048]{1,0:T(8,128)(2,1)}), bf16[384,8192]{1,0:T(8,128)(2,1)}) %all-gather.9.cloned.1.call-update) | async-done | bytes 6291472 | tf_op jit(solution)/shard_map/all_gather | solution.py:58
  111.3 6.5 copy.32
  117.8 95.9 %all-to-all-done = bf16[384,8,1024]{2,0,1:T(8,128)(2,1)} async-done(((bf16[384,8,1024]{2,0,1:T(8,128)(2,1)}), bf16[384,8,1024]{2,0,1:T(8,128)(2,1)}, u32[]{:S(2)}, u32[]{:S(2)}) %all-to-all-start) | async-done | bytes 6291488 | tf_op jit(solution)/shard_map/all_to_all | solution.py:65
  219.0 6.5 copy.31
  225.5 130.6 %all-to-all-done.1 = bf16[384,8,1024]{2,0,1:T(8,128)(2,1)} async-done(((bf16[384,8,1024]{2,0,1:T(8,128)(2,1)}), bf16[384,8,1024]{2,0,1:T(8,128)(2,1)}, u32[]{:S(2)}, u32[]{:S(2)}) %all-to-all-start.1) | async-done | bytes 6291488 | tf_op jit(solution)/shard_map/all_to_all | solution.py:66
  356.1 5.0 all-to-all-start.2
  362.6 6.5 copy.30
  369.1 129.3 %all-to-all-done.2 = bf16[384,8,1024]{2,0,1:T(8,128)(2,1)} async-done(((bf16[384,8,1024]{2,0,1:T(8,128)(2,1)}), bf16[384,8,1024]{2,0,1:T(8,128)(2,1)}, u32[]{:S(2)}, u32[]{:S(2)}) %all-to-all-start.2) | async-done | bytes 6291488 | tf_op jit(solution)/shard_map/all_to_all | solution.py:67
  510.2 7.6 fusion.7
  519.4 86.6 %collective-permute-done = f32[128,3072]{1,0:T(8,128)S(1)} collective-permute-done((f32[128,3072]{1,0:T(8,128)S(1)}, f32[128,3072]{1,0:T(8,128)S(1)}, u32[]{:S(2)}, u32[]{:S(2)}) %collective-permute-start) | collective-permute-done | bytes 1572896 | tf_op jit(solution)/shard_map/ppermute | solution.py:14
  606.4 66.6 %collective-permute-done.1 = f32[128,3072]{1,0:T(8,128)S(1)} collective-permute-done((f32[128,3072]{1,0:T(8,128)S(1)}, f32[128,3072]{1,0:T(8,128)S(1)}, u32[]{:S(2)}, u32[]{:S(2)}) %collective-permute-start.1) | collective-permute-done | bytes 1572896 | tf_op jit(solution)/shard_map/ppermute | solution.py:14
  675.0 68.3 %collective-permute-done.2 = f32[128,3072]{1,0:T(8,128)S(1)} collective-permute-done((f32[128,3072]{1,0:T(8,128)S(1)}, f32[128,3072]{1,0:T(8,128)S(1)}, u32[]{:S(2)}, u32[]{:S(2)}) %collective-permute-start.2) | collective-permute-done | bytes 1572896 | tf_op jit(solution)/shard_map/ppermute | solution.py:14
  748.0 6.7 fusion.20
  754.7 34.6 %collective-permute-done.3 = f32[128,3072]{1,0:T(8,128)S(1)} collective-permute-done((f32[128,3072]{1,0:T(8,128)S(1)}, f32[128,3072]{1,0:T(8,128)S(1)}, u32[]{:S(2)}, u32[]{:S(2)}) %collective-permute-start.3) | collective-permute-done | bytes 1572896 | tf_op jit(solution)/shard_map/ppermute | solution.py:14
  792.1 33.7 %collective-permute-done.4 = f32[128,3072]{1,0:T(8,128)S(1)} collective-permute-done((f32[128,3072]{1,0:T(8,128)S(1)}, f32[128,3072]{1,0:T(8,128)S(1)}, u32[]{:S(2)}, u32[]{:S(2)}) %collective-permute-start.4) | collective-permute-done | bytes 1572896 | tf_op jit(solution)/shard_map/ppermute | solution.py:14
  829.4 66.8 %collective-permute-done.5 = f32[128,3072]{1,0:T(8,128)S(1)} collective-permute-done((f32[128,3072]{1,0:T(8,128)S(1)}, f32[128,3072]{1,0:T(8,128)S(1)}, u32[]{:S(2)}, u32[]{:S(2)}) %collective-permute-start.5) | collective-permute-done | bytes 1572896 | tf_op jit(solution)/shard_map/ppermute | solution.py:14
  897.8 6.4 copy.40
  904.2 6.3 copy.41
  913.3 6.4 copy.43
  919.6 6.3 copy.44
  (69 shorter events, 47.4 us)
Async XLA Ops:
  7.2 55.6 %all-gather.7.cloned.1.call-start = ((), (), s32[]{:S(2)}) async-start(), calls=%async_computation.4 | async-start | bytes 7864320 | tf_op jit(solution)/shard_map/all_gather | solution.py:57
  13.5 97.8 %all-gather.9.cloned.1.call-start = ((), (), s32[]{:S(2)}) async-start(), calls=%async_computation.5 | async-start | bytes 7864320 | tf_op jit(solution)/shard_map/all_gather | solution.py:58
  69.2 6.6 copy-start.1
  69.2 144.4 %all-to-all-start = ((bf16[384,8,1024]{2,0,1:T(8,128)(2,1)}), bf16[384,8,1024]{2,0,1:T(8,128)(2,1)}, u32[]{:S(2)}, u32[]{:S(2)}) async-start(bf16[384,8,1024]{2,0,1:T(8,128)(2,1)} %bitcast.39), calls=%async_computation | async-start | bytes 12582912 | tf_op jit(solution)/shard_map/all_to_all | solution.py:65
  75.0 144.0 %all-gather.13.cloned.1.call-start = ((), (), s32[]{:S(2)}) async-start(), calls=%async_computation.7 | async-start | bytes 7864320 | tf_op jit(solution)/shard_map/all_gather | solution.py:60
  213.7 142.5 %all-to-all-start.1 = ((bf16[384,8,1024]{2,0,1:T(8,128)(2,1)}), bf16[384,8,1024]{2,0,1:T(8,128)(2,1)}, u32[]{:S(2)}, u32[]{:S(2)}) async-start(bf16[384,8,1024]{2,0,1:T(8,128)(2,1)} %bitcast.40), calls=%async_computation.1 | async-start | bytes 12582912 | tf_op jit(solution)/shard_map/all_to_all | solution.py:66
  218.4 144.2 %all-gather.15.cloned.1.call-start = ((), (), s32[]{:S(2)}) async-start(), calls=%async_computation.8 | async-start | bytes 7864320 | tf_op jit(solution)/shard_map/all_gather | solution.py:61
  356.1 142.3 %all-to-all-start.2 = ((bf16[384,8,1024]{2,0,1:T(8,128)(2,1)}), bf16[384,8,1024]{2,0,1:T(8,128)(2,1)}, u32[]{:S(2)}, u32[]{:S(2)}) async-start(bf16[384,8,1024]{2,0,1:T(8,128)(2,1)} %bitcast.41), calls=%async_computation.2 | async-start | bytes 12582912 | tf_op jit(solution)/shard_map/all_to_all | solution.py:67
  361.1 149.0 %all-gather.11.cloned.1.call-start = ((), (), s32[]{:S(2)}) async-start(), calls=%async_computation.6 | async-start | bytes 7864320 | tf_op jit(solution)/shard_map/all_gather | solution.py:59
  498.4 5.3 copy-start.3
  498.4 249.6 %all-to-all-start.3 = ((bf16[384,8,1024]{2,0,1:T(8,128)(2,1)}), bf16[384,8,1024]{2,0,1:T(8,128)(2,1)}, u32[]{:S(2)}, u32[]{:S(2)}) async-start(bf16[384,8,1024]{2,0,1:T(8,128)(2,1)} %bitcast.38), calls=%async_computation.3 | async-start | bytes 12582912 | tf_op jit(solution)/shard_map/all_to_all | solution.py:68
  503.4 244.6 %all-gather.17.cloned.1.call-start = ((), (), s32[]{:S(2)}) async-start(), calls=%async_computation.9 | async-start | bytes 7864320 | tf_op jit(solution)/shard_map/all_gather | solution.py:62
  517.9 88.2 %collective-permute-start = (f32[128,3072]{1,0:T(8,128)S(1)}, f32[128,3072]{1,0:T(8,128)S(1)}, u32[]{:S(2)}, u32[]{:S(2)}) collective-permute-start(f32[128,3072]{1,0:T(8,128)S(1)} %fusion.7), channel_id=1, source_target_pairs={{0,4},{4,0},{8,12},{12,8},{16,20},{20,16},{24,28},{28,24},{1,5},{5... | collective-permute-start | bytes 4718600 | tf_op jit(solution)/shard_map/ppermute | solution.py:14
  606.3 66.7 %collective-permute-start.1 = (f32[128,3072]{1,0:T(8,128)S(1)}, f32[128,3072]{1,0:T(8,128)S(1)}, u32[]{:S(2)}, u32[]{:S(2)}) collective-permute-start(f32[128,3072]{1,0:T(8,128)S(1)} %add.70), channel_id=1, source_target_pairs={{0,8},{4,12},{8,0},{12,4},{16,24},{20,28},{24,16},{28,20},{1,9},{5... | collective-permute-start | bytes 4718600 | tf_op jit(solution)/shard_map/ppermute | solution.py:14
  673.2 70.5 %copy-start.4 = (f32[3072]{0:T(1024)S(1)}, f32[3072]{0:T(1024)}, u32[]{:S(2)}) copy-start(f32[3072]{0:T(1024)} %param.19) | copy-start | bytes 36868
  673.2 70.1 %collective-permute-start.2 = (f32[128,3072]{1,0:T(8,128)S(1)}, f32[128,3072]{1,0:T(8,128)S(1)}, u32[]{:S(2)}, u32[]{:S(2)}) collective-permute-start(f32[128,3072]{1,0:T(8,128)S(1)} %add.71), channel_id=1, source_target_pairs={{0,16},{4,20},{8,24},{12,28},{16,0},{20,4},{24,8},{28,12},{1,17},{... | collective-permute-start | bytes 4718600 | tf_op jit(solution)/shard_map/ppermute | solution.py:14
  754.7 34.7 %collective-permute-start.3 = (f32[128,3072]{1,0:T(8,128)S(1)}, f32[128,3072]{1,0:T(8,128)S(1)}, u32[]{:S(2)}, u32[]{:S(2)}) collective-permute-start(f32[128,3072]{1,0:T(8,128)S(1)} %fusion.20), channel_id=1, source_target_pairs={{0,4},{4,0},{8,12},{12,8},{16,20},{20,16},{24,28},{28,24},{1,5},{5... | collective-permute-start | bytes 4718600 | tf_op jit(solution)/shard_map/ppermute | solution.py:14
  789.6 36.2 %collective-permute-start.4 = (f32[128,3072]{1,0:T(8,128)S(1)}, f32[128,3072]{1,0:T(8,128)S(1)}, u32[]{:S(2)}, u32[]{:S(2)}) collective-permute-start(f32[128,3072]{1,0:T(8,128)S(1)} %add.77), channel_id=1, source_target_pairs={{0,8},{4,12},{8,0},{12,4},{16,24},{20,28},{24,16},{28,20},{1,9},{5... | collective-permute-start | bytes 4718600 | tf_op jit(solution)/shard_map/ppermute | solution.py:14
  826.0 70.6 %copy-start.5 = (f32[3072]{0:T(1024)S(1)}, f32[3072]{0:T(1024)}, u32[]{:S(2)}) copy-start(f32[3072]{0:T(1024)} %param.21) | copy-start | bytes 36868
  826.0 70.3 %collective-permute-start.5 = (f32[128,3072]{1,0:T(8,128)S(1)}, f32[128,3072]{1,0:T(8,128)S(1)}, u32[]{:S(2)}, u32[]{:S(2)}) collective-permute-start(f32[128,3072]{1,0:T(8,128)S(1)} %add.78), channel_id=1, source_target_pairs={{0,16},{4,20},{8,24},{12,28},{16,0},{20,4},{24,8},{28,12},{1,17},{... | collective-permute-start | bytes 4718600 | tf_op jit(solution)/shard_map/ppermute | solution.py:14
  897.8 12.7 %slice-start = ((s8[6291456]{0:T(1024)(128)(4,1)}), s8[4194304]{0:T(1024)(128)(4,1)S(1)}, s32[]{:S(2)}) async-start(s8[6291456]{0:T(1024)(128)(4,1)} %bitcast.34), calls=%async_computation.10 | async-start | bytes 8388608
  904.2 6.4 slice-start.1
  913.3 12.7 %slice-start.2 = ((s8[6291456]{0:T(1024)(128)(4,1)}), s8[4194304]{0:T(1024)(128)(4,1)S(1)}, s32[]{:S(2)}) async-start(s8[6291456]{0:T(1024)(128)(4,1)} %bitcast.36), calls=%async_computation.12 | async-start | bytes 8388608
  919.6 6.4 slice-start.3
  (2 other events, 6.2 us)
Sparse Core Ops, SparseCore 0:
  13.6 49.0 all-gather.6
  64.9 46.3 all-gather.8
  113.4 46.3 all-gather.12
  221.0 46.7 all-gather.14
  363.8 46.7 all-gather.10
  506.1 46.7 all-gather.16
